TPU v7x, 512 devices: a whole 4x4x16 slice. The times are simulated.
512 devices in a mesh: sp: 16 (over z), fs: 4 (over y), tp: 8 (over x, core).
Axes of the slice: x: 4, y: 4, z: 16, core: 2. Of those that a mesh axis runs over, the one named last changes fastest.
Arguments:
- tokens: bfloat16 [4, 4096, 2048], P('fs', ('sp', 'tp')), may hold values from -6 to 6
- query_weight: bfloat16 [2048, 2048], P(('sp', 'fs'), 'tp'), may hold values from -0.125 to 0.125
- forget_weight: bfloat16 [2048, 2048], P(('sp', 'fs'), 'tp'), may hold values from -0.125 to 0.125
- value_weight: bfloat16 [2048, 2048], P(('sp', 'fs'), 'tp'), may hold values from -0.125 to 0.125
- convolution_gate_weight: bfloat16 [2048, 1024], P(('sp', 'fs'), 'tp'), may hold values from -0.125 to 0.125
- convolution_multiplier_weight: bfloat16 [2048, 1024], P(('sp', 'fs'), 'tp'), may hold values from -0.125 to 0.125
- convolution_input_weight: bfloat16 [2048, 1024], P(('sp', 'fs'), 'tp'), may hold values from -0.125 to 0.125
- gate_headroom: float32 [2048], P('tp'), may hold values from 2.4414063e-05 to 0.06
- added_log_rate: float32 [4, 16, 4096], P('fs', 'tp', 'sp'), may hold values from -1.6 to 0
- initial_state: float32 [4, 16, 128, 128], P('fs', 'tp'), may hold values from -0.25 to 0.25
- head_norm_gain: float32 [2048], P('tp'), may hold values from 0.1 to 1.9
- convolution_taps: float32 [3, 1024], P(None, 'tp'), may hold values from -3.5 to 3.5
- convolution_bias: float32 [1024], P('tp'), may hold values from -4 to 4
- recurrence_output_weight: bfloat16 [2048, 2048], P('tp', ('sp', 'fs')), may hold values from -0.109375 to 0.109375
- convolution_output_weight: bfloat16 [1024, 2048], P('tp', ('sp', 'fs')), may hold values from -0.109375 to 0.109375
Outputs:
- mixed: bfloat16 [4, 4096, 2048], P('fs', ('sp', 'tp'))
All inputs are finite; a program needn't handle non-finite values.
Results may differ from a plain program's by a relative error of at most 0.018.
Values may be sent and summed in bfloat16 or wider, within the bound.
A program may use at most 64 MiB of HBM per device.

v0:
```python
import jax
import jax.numpy as jnp
from jax import lax
from jax.sharding import PartitionSpec as P

DK = 128
KW = 3
BLOCK_POSITIONS = 64


def gather_turned(arrays, axis, dims):
    turned = [jnp.moveaxis(a, dim, 0) for a, dim in zip(arrays, dims)]
    widths = [t[0].size for t in turned]
    both = jnp.concatenate([t.reshape(-1, w) for t, w in zip(turned, widths)], axis=1)
    result = lax.all_gather(both, axis, axis=0, tiled=True)
    parts = jnp.split(result, [sum(widths[:k]) for k in range(1, len(widths))], axis=1)
    return tuple(
        (
            jnp.moveaxis(b.reshape(-1, *t.shape[1:]), 0, dim)
            for b, t, dim in zip(parts, turned, dims)
        )
    )


def copy_for_each(value, axis):
    copies = jnp.broadcast_to(value, (lax.axis_size(axis), *value.shape))
    return lax.all_to_all(copies, axis, split_axis=0, concat_axis=0, tiled=True)


def in_order(parts, dim):
    parts = jnp.moveaxis(parts, 0, dim)
    dims = parts.shape
    return parts.reshape(*dims[:dim], dims[dim] * dims[dim + 1], *dims[dim + 2 :])


def gather_directly(value, axis, dim):
    parts = copy_for_each(value, axis)
    return in_order(parts, dim)


def carried_in(part, axis, combine, identity):
    place = lax.axis_index(axis)
    gathered = jax.tree.map(lambda a: lax.all_gather(a, axis), part)
    state = jax.tree.map(lambda a, e: jnp.zeros_like(a) + jnp.asarray(e, a.dtype), part, identity)

    def one(hop, state):
        return combine(
            state, jax.tree.map(lambda a: lax.dynamic_index_in_dim(a, hop, 0, False), gathered)
        )

    return lax.fori_loop(0, place, one, state)


def from_behind(block, axis, distance):
    devices = range(lax.axis_size(axis))
    route = [(i - distance, i) for i in devices if i - distance in devices]
    return lax.ppermute(block, axis, route)


def in_blocks(value, dim, peers):
    before, after = (value.shape[:dim], value.shape[dim + 1 :])
    return jnp.moveaxis(value.reshape(*before, peers, -1, *after), dim, 0)


def summed_on_arrival(value, axis, dim):
    parts = in_blocks(value, dim, lax.axis_size(axis))
    arrived = lax.all_to_all(parts, axis, split_axis=0, concat_axis=0, tiled=True)
    return arrived.astype(jnp.float32).sum(axis=0)


def to_blocks(values, number_of_heads):
    number_of_blocks = values.shape[0] // BLOCK_POSITIONS
    return jnp.transpose(
        values.reshape(number_of_blocks, BLOCK_POSITIONS, number_of_heads, DK), (2, 0, 1, 3)
    )


def within_block_recurrence(
    query_vectors, forget_logits, value_vectors, gate_headroom, extra_rates
):
    number_of_heads = extra_rates.shape[0]
    number_of_blocks = query_vectors.shape[0] // BLOCK_POSITIONS
    query_scaled = to_blocks(query_vectors.astype(jnp.float32), number_of_heads) * DK ** (-0.5)
    gated_key = to_blocks(
        gate_headroom[None, :] * jax.nn.sigmoid(-forget_logits.astype(jnp.float32)), number_of_heads
    )
    forget_log_rate = (
        jnp.log1p(-gated_key)
        + extra_rates.reshape(number_of_heads, number_of_blocks, BLOCK_POSITIONS)[..., None]
    )
    values = to_blocks(value_vectors.astype(jnp.float32), number_of_heads)
    cumulative = jnp.cumsum(forget_log_rate, axis=2)
    query_decayed = query_scaled * jnp.exp(cumulative)
    key_decayed = gated_key * jnp.exp(-cumulative)
    scores = jnp.einsum("hnik,hnjk->hnij", query_decayed, key_decayed)
    causal = jnp.tril(jnp.ones((BLOCK_POSITIONS, BLOCK_POSITIONS), dtype=bool))
    scores = jnp.where(causal, scores, 0.0)
    within = jnp.einsum("hnij,hnjv->hniv", scores, values)
    final_log = cumulative[:, :, -1, :]
    contrib = jnp.einsum(
        "hnck,hncv->hnkv", gated_key * jnp.exp(final_log[:, :, None, :] - cumulative), values
    )
    decays = jnp.exp(final_log)

    def advance(current, block_pair):
        return (block_pair[0][..., None] * current + block_pair[1], current)

    empty_state = jnp.zeros((number_of_heads, DK, DK), jnp.float32)
    local_total, entering = lax.scan(
        advance, empty_state, (jnp.moveaxis(decays, 1, 0), jnp.moveaxis(contrib, 1, 0))
    )
    entering = jnp.moveaxis(entering, 0, 1)
    before = jnp.exp(jnp.cumsum(final_log, axis=1) - final_log)
    device_decay = jnp.exp(jnp.sum(final_log, axis=1))
    return (query_decayed, within, entering, before, device_decay, local_total)


def finish(query_decayed, within, entering, before, carried, head_norm_gain):
    number_of_heads = query_decayed.shape[0]
    states = entering + before[..., None] * carried[:, None]
    carried_term = jnp.einsum("hnck,hnkv->hncv", query_decayed, states)
    length = query_decayed.shape[1] * BLOCK_POSITIONS
    recurrence_unnormed = jnp.transpose(within + carried_term, (1, 2, 0, 3)).reshape(
        length, number_of_heads, DK
    )
    mean_square = jnp.mean(recurrence_unnormed * recurrence_unnormed, axis=-1, keepdims=True)
    rec_out = (
        recurrence_unnormed
        * lax.rsqrt(mean_square + 1e-06)
        * head_norm_gain.reshape(number_of_heads, DK)
    )
    return rec_out.reshape(length, number_of_heads * DK).astype(jnp.bfloat16)


def chain_combine(earlier_part, later_part):
    return (
        earlier_part[0] * later_part[0],
        later_part[0][..., None] * earlier_part[1] + later_part[1],
    )


def shards(
    tokens,
    query_weight,
    forget_weight,
    value_weight,
    convolution_gate_weight,
    convolution_multiplier_weight,
    convolution_input_weight,
    gate_headroom,
    added_log_rate,
    initial_state,
    head_norm_gain,
    convolution_taps,
    convolution_bias,
    recurrence_output_weight,
    convolution_output_weight,
):
    own_rows = tokens[0]
    gathered = gather_turned(
        (
            query_weight,
            forget_weight,
            value_weight,
            convolution_gate_weight,
            convolution_multiplier_weight,
            convolution_input_weight,
            recurrence_output_weight,
            convolution_output_weight,
        ),
        ("sp", "fs"),
        (0, 0, 0, 0, 0, 0, 1, 1),
    )
    in_weights = gathered[:6]
    out_rec = gathered[6]
    out_conv = gathered[7]
    block_rows = gather_directly(own_rows, "tp", 0)
    projected = jnp.concatenate(
        [
            jnp.dot(block_rows, weight, preferred_element_type=jnp.float32).astype(jnp.bfloat16)
            for weight in in_weights
        ],
        axis=1,
    )
    rec_width = query_weight.shape[1]
    conv_width = convolution_gate_weight.shape[1]
    query_vectors = projected[:, :rec_width]
    forget_logits = projected[:, rec_width : 2 * rec_width]
    value_vectors = projected[:, 2 * rec_width : 3 * rec_width]
    conv_base = 3 * rec_width
    conv_gate = projected[:, conv_base : conv_base + conv_width]
    conv_mult = projected[:, conv_base + conv_width : conv_base + 2 * conv_width]
    conv_input = projected[:, conv_base + 2 * conv_width : conv_base + 3 * conv_width]
    query_decayed, within, entering, before, device_decay, local_total = within_block_recurrence(
        query_vectors, forget_logits, value_vectors, gate_headroom, added_log_rate[0]
    )
    conv_prod = conv_mult.astype(jnp.float32) * conv_input.astype(jnp.float32)
    length = conv_prod.shape[0]
    tail_rows = conv_prod[length - (KW - 1) :]
    unit_decay = jnp.ones_like(device_decay)
    empty_state = jnp.zeros_like(local_total)
    prior_decay, prior_state = carried_in(
        (device_decay, local_total), "sp", chain_combine, (unit_decay, empty_state)
    )
    prior_rows = from_behind(tail_rows, "sp", 1)
    carried = prior_decay[..., None] * initial_state[0] + prior_state
    rec_out = finish(query_decayed, within, entering, before, carried, head_norm_gain)
    extended = jnp.concatenate([prior_rows, conv_prod], axis=0)
    conv_y = jnp.broadcast_to(convolution_bias[None, :], conv_prod.shape)
    for j in range(KW):
        conv_y = conv_y + convolution_taps[j][None, :] * extended[j : j + length]
    conv_out = (conv_gate.astype(jnp.float32) * conv_y).astype(jnp.bfloat16)
    mixed = summed_on_arrival(
        (
            jnp.dot(rec_out, out_rec, preferred_element_type=jnp.float32)
            + jnp.dot(conv_out, out_conv, preferred_element_type=jnp.float32)
        ).astype(jnp.bfloat16),
        "tp",
        0,
    )
    return mixed.astype(jnp.bfloat16)[None]


def solution(mesh):
    in_specs = (
        P("fs", ("sp", "tp"), None),
        P(("sp", "fs"), "tp"),
        P(("sp", "fs"), "tp"),
        P(("sp", "fs"), "tp"),
        P(("sp", "fs"), "tp"),
        P(("sp", "fs"), "tp"),
        P(("sp", "fs"), "tp"),
        P("tp"),
        P("fs", "tp", "sp"),
        P("fs", "tp", None, None),
        P("tp"),
        P(None, "tp"),
        P("tp"),
        P("tp", ("sp", "fs")),
        P("tp", ("sp", "fs")),
    )
    out_specs = P("fs", ("sp", "tp"), None)
    return jax.shard_map(shards, mesh=mesh, in_specs=in_specs, out_specs=out_specs, check_vma=False)
```

profile of v0, /device:TPU:488, one launch (start us, length us, event | category | flops | bytes accessed | tf_op | source)
XLA Modules:
  0.0 286.8 jit_solution(150869934221793700)
XLA Ops:
  12.9 2.0 broadcast_in_dim.41
  14.9 4.3 %all-to-all-start = ((bf16[8,32,2048]{2,1,0:T(8,128)(2,1)}), bf16[8,32,2048]{2,1,0:T(8,128)(2,1)S(1)}, u32[]{:S(2)}, u32[]{:S(2)}) async-start(bf16[8,32,2048]{2,1,0:T(8,128)(2,1)} %broadcast_in_dim.41), calls=%async_computation | async-start | bytes 2097152 | tf_op jit(solution)/shard_map/all_to_all | solution.py:27
  20.0 15.1 %all-to-all-done = bf16[8,32,2048]{2,1,0:T(8,128)(2,1)S(1)} async-done(((bf16[8,32,2048]{2,1,0:T(8,128)(2,1)}), bf16[8,32,2048]{2,1,0:T(8,128)(2,1)S(1)}, u32[]{:S(2)}, u32[]{:S(2)}) %all-to-all-start) | async-done | bytes 1048608 | tf_op jit(solution)/shard_map/all_to_all | solution.py:27
  35.2 125.2 %all-gather.6.cloned.1.call-done = bf16[2048,1536]{1,0:T(8,128)(2,1)} async-done(((bf16[32,1536]{1,0:T(8,128)(2,1)}), bf16[2048,1536]{1,0:T(8,128)(2,1)}) %all-gather.6.cloned.1.call-update) | async-done | bytes 6291472 | tf_op jit(solution)/shard_map/all_gather | solution.py:15
  160.4 1.7 fusion.8
  163.0 1.7 fusion.12
  166.7 1.7 fusion.11
  168.8 1.5 fusion.16
  170.4 1.5 fusion.15
  172.0 1.3 collective-permute-start
  173.3 27.9 %all-gather.2 = f32[16,2,128]{2,1,0:T(2,128)S(1)} all-gather(f32[1,2,128]{2,1,0:T(2,128)S(1)} %exponential_bitcast_fusion.1), channel_id=2, replica_groups=mesh['sp'=16,'fs'=4,'tp'=8] {'sp'}, dimensions={0}, use_global_device_ids=true | all-gather | bytes 17408 | tf_op jit(solution)/shard_map/all_gather | solution.py:43
  201.5 34.2 %all-gather.8.cloned.1.call-done = f32[32,128,128]{2,1,0:T(8,128)} async-done(((f32[2,128,128]{2,1,0:T(8,128)}), f32[32,128,128]{2,1,0:T(8,128)}) %all-gather.8.cloned.1.call-update) | async-done | bytes 2097168 | tf_op jit(solution)/shard_map/all_gather | solution.py:43
  235.7 16.2 %while.25 = (s32[]{:T(128)}, f32[2,128]{1,0:T(2,128)S(1)}, f32[2,128,128]{2,1,0:T(8,128)S(1)}, s32[]{:T(128)}, f32[16,2,128]{2,1,0:T(2,128)S(1)}, /*index=5*/f32...) while((s32[]{:T(128)}, f32[2,128]{1,0:T(2,128)S(1)}, f32[2,128,128]{2,1,0:T(8,128)S(1)}, s32[]{:T(128)}, ...), condition=%wide.region_6.7_spmd, body=%wide.region_5.6_spmd.sunk | while | flops 65797 | bytes 398471 | solution.py:51
  235.7 1.0 bitcast_add_fusion.7
  236.8 1.0 bitcast_add_fusion.7
  237.9 1.0 bitcast_add_fusion.7
  239.0 1.0 bitcast_add_fusion.7
  240.0 1.0 bitcast_add_fusion.7
  241.1 1.0 bitcast_add_fusion.7
  242.2 1.0 bitcast_add_fusion.7
  243.3 1.0 bitcast_add_fusion.7
  244.3 1.0 bitcast_add_fusion.7
  245.4 1.0 bitcast_add_fusion.7
  246.5 1.0 bitcast_add_fusion.7
  247.6 1.0 bitcast_add_fusion.7
  248.6 1.0 bitcast_add_fusion.7
  249.7 1.0 bitcast_add_fusion.7
  250.8 1.0 bitcast_add_fusion.7
  253.1 1.7 fusion.19
  254.8 3.7 %fusion = bf16[256,2048]{1,0:T(8,128)(2,1)} fusion(f32[256,2048]{1,0:T(8,128)S(1)} %fusion.19, bf16[2048,1536]{1,0:T(8,128)(2,1)} %all-gather.6.cloned.1.call-done, f32[2,128]{0,1:T(8,128)S(1)} %collective-permute-done, f32[256,128]{0,1:T(8,128)S(1)} %fusion.15, bf16[256,2048]{1,0:T(8,128)(2,1)S(1)} %bitcast.116, f32[128]{0:T(128)S(1)} %get-tuple-element.133, ...), kind=kOutput, calls=%fused_computation.6 | convolution fusion | flops 269877248 | bytes 5377024 | tf_op jit(solution)/shard_map/dot_general | solution.py:216
  258.5 20.6 %all_to_all.10 = bf16[8,32,2048]{2,1,0:T(8,128)(2,1)S(1)} all-to-all(bf16[8,32,2048]{2,1,0:T(8,128)(2,1)} %bitcast.117), channel_id=1, replica_groups=mesh['sp'=16,'fs'=4,'tp'=8] {'tp'}, dimensions={0} | all-to-all | bytes 2097152 | tf_op jit(solution)/shard_map/all_to_all | solution.py:67
  279.1 0.8 reduce_sum.32
  (80 shorter events, 12.7 us)
Async XLA Ops:
  6.5 153.9 %all-gather.6.cloned.1.call-start = ((), (), s32[]{:S(2)}) async-start(), calls=%async_computation.2 | async-start | bytes 6389760 | tf_op jit(solution)/shard_map/all_gather | solution.py:15
  12.2 0.6 copy-start.1
  14.9 20.2 %all-to-all-start = ((bf16[8,32,2048]{2,1,0:T(8,128)(2,1)}), bf16[8,32,2048]{2,1,0:T(8,128)(2,1)S(1)}, u32[]{:S(2)}, u32[]{:S(2)}) async-start(bf16[8,32,2048]{2,1,0:T(8,128)(2,1)} %broadcast_in_dim.41), calls=%async_computation | async-start | bytes 2097152 | tf_op jit(solution)/shard_map/all_to_all | solution.py:27
  19.2 216.4 %all-gather.8.cloned.1.call-start = ((), (), s32[]{:S(2)}) async-start(), calls=%async_computation.3 | async-start | bytes 2228224 | tf_op jit(solution)/shard_map/all_gather | solution.py:43
  160.4 6.3 %copy-start.3 = (f32[3,128]{1,0:T(4,128)S(1)}, f32[3,128]{1,0:T(4,128)}, u32[]{:S(2)}) copy-start(f32[3,128]{1,0:T(4,128)} %param.30) | copy-start | bytes 4612
  165.9 0.7 copy-start
  165.9 85.9 %copy-start.2 = (f32[1,2,128,128]{3,2,1,0:T(8,128)S(1)}, f32[1,2,128,128]{3,2,1,0:T(8,128)}, u32[]{:S(2)}) copy-start(f32[1,2,128,128]{3,2,1,0:T(8,128)} %param.28) | copy-start | bytes 393220
  168.4 84.7 %copy-start.4 = (f32[256]{0:T(256)S(1)}, f32[256]{0:T(256)}, u32[]{:S(2)}) copy-start(f32[256]{0:T(256)} %param.29) | copy-start | bytes 3076
  172.0 82.8 %collective-permute-start = (f32[2,128]{0,1:T(8,128)S(1)}, f32[2,128]{0,1:T(8,128)S(1)}, u32[]{:S(2)}, u32[]{:S(2)}) collective-permute-start(f32[2,128]{0,1:T(8,128)S(1)} %slice.29), channel_id=1, source_target_pairs={{0,32},{32,64},{64,96},{96,128},{128,160},{160,192},{192,224},{224... | collective-permute-start | bytes 3080 | tf_op jit(solution)/shard_map/ppermute | solution.py:57
Sparse Core Ops, SparseCore 0:
  13.0 147.3 all-gather.5
  166.7 68.8 all-gather.7
where the time goes:
time: 288 us; the launch traced here: 287 us
  waiting for transfers between devices  175 us (61%)
  blocking collectives  48.5 us (17%)
  other arithmetic  17.6 us (6%)
  matrix products  14.6 us (5%)
  between operations  13.7 us (5%)
  local copies, waits for them, and re-layouts  11.5 us (4%)
  starting transfers between devices  5.63 us (2%)
    all_gather x1, waiting for transfers between devices, gather_turned(): result = lax.all_gather(both, axis, axis=0, tiled=True)  125 us
    all_gather x1, waiting for transfers between devices, carried_in(): gathered = jax.tree.map(lambda a: lax.all_gather(a, axis), part)  34.2 us
    all_gather x1, blocking collectives, carried_in(): gathered = jax.tree.map(lambda a: lax.all_gather(a, axis), part)  27.9 us
    all_to_all x1, blocking collectives, summed_on_arrival(): lax.all_to_all(parts, axis, split_axis=0, concat_axis=0, tiled=True)  20.6 us
    add x15, other arithmetic, chain_combine(): later_part[0][..., None] * earlier_part[1] + later_part[1]  15.4 us
    all_to_all x1, waiting for transfers between devices, copy_for_each(): return lax.all_to_all(copies, axis, split_axis=0, concat_axis=0, tiled=True)  15.1 us
    dot_general x5, matrix products, shards(): jnp.dot(block_rows, weight, preferred_element_type=jnp.float32)  8.2 us
    unnamed x18, local copies, waits for them, and re-layouts  6.28 us
  transfers between devices with their start and end apart: 4, of which 3 were waited for; matrix products, arithmetic and copies ran while one was open for 9% of the time, Pallas kernels for 0%

commit v1 on v0

--- a/solution.py
+++ b/solution.py
@@ -12,7 +12,10 @@
     turned = [jnp.moveaxis(a, dim, 0) for a, dim in zip(arrays, dims)]
     widths = [t[0].size for t in turned]
     both = jnp.concatenate([t.reshape(-1, w) for t, w in zip(turned, widths)], axis=1)
-    result = lax.all_gather(both, axis, axis=0, tiled=True)
+    peers_2 = lax.axis_size(axis)
+    shards_2 = jnp.stack([both for _ in range(peers_2)])
+    shards_2 = lax.all_to_all(shards_2, axis, split_axis=0, concat_axis=0)
+    result = jnp.concatenate(shards_2, axis=0)
     parts = jnp.split(result, [sum(widths[:k]) for k in range(1, len(widths))], axis=1)
     return tuple(
         (

time: 288 us -> 445 us (1.55)
  the two profiles are of different devices: /device:TPU:488 before, /device:TPU:480 now
where the time goes in v1:
time: 445 us; the launch traced here: 444 us
  waiting for transfers between devices  311 us (70%)
  blocking collectives  53.9 us (12%)
  starting transfers between devices  18.2 us (4%)
  other arithmetic  17.6 us (4%)
  matrix products  14.7 us (3%)
  local copies, waits for them, and re-layouts  14.2 us (3%)
  between operations  13.7 us (3%)
    all_to_all x1, waiting for transfers between devices, gather_turned(): shards_2 = lax.all_to_all(shards_2, axis, split_axis=0, concat_axis=0)  272 us
    all_gather x1, blocking collectives, carried_in(): gathered = jax.tree.map(lambda a: lax.all_gather(a, axis), part)  33.1 us
    all_gather x1, waiting for transfers between devices, carried_in(): gathered = jax.tree.map(lambda a: lax.all_gather(a, axis), part)  28.8 us
    all_to_all x1, blocking collectives, summed_on_arrival(): lax.all_to_all(parts, axis, split_axis=0, concat_axis=0, tiled=True)  20.9 us
    add x15, other arithmetic, chain_combine(): later_part[0][..., None] * earlier_part[1] + later_part[1]  15.4 us
    all_to_all x1, starting transfers between devices, gather_turned(): shards_2 = lax.all_to_all(shards_2, axis, split_axis=0, concat_axis=0)  12.6 us
    all_to_all x1, waiting for transfers between devices, copy_for_each(): return lax.all_to_all(copies, axis, split_axis=0, concat_axis=0, tiled=True)  10.2 us
  transfers between devices with their start and end apart: 4, of which 3 were waited for; matrix products, arithmetic and copies ran while one was open for 7% of the time, Pallas kernels for 0%

profile of v1, /device:TPU:480, one launch (start us, length us, event | category | flops | bytes accessed | tf_op | source)
XLA Modules:
  0.0 444.0 jit_solution(13738647609879659848)
XLA Ops:
  6.5 2.0 broadcast_in_dim.41
  8.5 4.3 all-to-all-start.1
  18.5 10.2 %all-to-all-done.1 = bf16[8,32,2048]{2,1,0:T(8,128)(2,1)S(1)} async-done(((bf16[8,32,2048]{2,1,0:T(8,128)(2,1)}), bf16[8,32,2048]{2,1,0:T(8,128)(2,1)S(1)}, u32[]{:S(2)}, u32[]{:S(2)}) %all-to-all-start.1) | async-done | bytes 1048608 | tf_op jit(solution)/shard_map/all_to_all | solution.py:30
  28.8 3.4 stack.2
  32.2 12.6 %all-to-all-start = ((bf16[64,32,1536]{2,1,0:T(8,128)(2,1)}), bf16[64,32,1536]{2,1,0:T(8,128)(2,1)}, u32[]{:S(2)}, u32[]{:S(2)}) async-start(bf16[64,32,1536]{2,1,0:T(8,128)(2,1)} %stack.2), calls=%async_computation | async-start | bytes 12582912 | tf_op jit(solution)/shard_map/all_to_all | solution.py:17
  44.9 272.0 %all-to-all-done = bf16[64,32,1536]{2,1,0:T(8,128)(2,1)} async-done(((bf16[64,32,1536]{2,1,0:T(8,128)(2,1)}), bf16[64,32,1536]{2,1,0:T(8,128)(2,1)}, u32[]{:S(2)}, u32[]{:S(2)}) %all-to-all-start) | async-done | bytes 6291488 | tf_op jit(solution)/shard_map/all_to_all | solution.py:17
  317.0 1.7 fusion.12
  318.7 1.7 fusion.8
  323.2 1.7 fusion.11
  325.4 1.5 fusion.16
  326.9 1.5 fusion.15
  329.2 1.3 collective-permute-start
  330.5 33.1 %all-gather.2 = f32[16,2,128]{2,1,0:T(2,128)S(1)} all-gather(f32[1,2,128]{2,1,0:T(2,128)S(1)} %exponential_bitcast_fusion.1), channel_id=2, replica_groups=mesh['sp'=16,'fs'=4,'tp'=8] {'sp'}, dimensions={0}, use_global_device_ids=true | all-gather | bytes 17408 | tf_op jit(solution)/shard_map/all_gather | solution.py:46
  363.9 28.8 %all-gather.5.cloned.1.call-done = f32[32,128,128]{2,1,0:T(8,128)} async-done(((f32[2,128,128]{2,1,0:T(8,128)}), f32[32,128,128]{2,1,0:T(8,128)}) %all-gather.5.cloned.1.call-update) | async-done | bytes 2097168 | tf_op jit(solution)/shard_map/all_gather | solution.py:46
  392.6 16.2 %while.25 = (s32[]{:T(128)}, f32[2,128]{1,0:T(2,128)S(1)}, f32[2,128,128]{2,1,0:T(8,128)S(1)}, s32[]{:T(128)}, f32[16,2,128]{2,1,0:T(2,128)S(1)}, /*index=5*/f32...) while((s32[]{:T(128)}, f32[2,128]{1,0:T(2,128)S(1)}, f32[2,128,128]{2,1,0:T(8,128)S(1)}, s32[]{:T(128)}, ...), condition=%wide.region_6.7_spmd, body=%wide.region_5.6_spmd.sunk | while | flops 65797 | bytes 398471 | solution.py:54
  392.7 1.0 bitcast_add_fusion.7
  393.8 1.0 bitcast_add_fusion.7
  394.8 1.0 bitcast_add_fusion.7
  395.9 1.0 bitcast_add_fusion.7
  397.0 1.0 bitcast_add_fusion.7
  398.1 1.0 bitcast_add_fusion.7
  399.1 1.0 bitcast_add_fusion.7
  400.2 1.0 bitcast_add_fusion.7
  401.3 1.0 bitcast_add_fusion.7
  402.4 1.0 bitcast_add_fusion.7
  403.4 1.0 bitcast_add_fusion.7
  404.5 1.0 bitcast_add_fusion.7
  406.7 1.0 bitcast_add_fusion.7
  407.8 1.0 bitcast_add_fusion.7
  410.1 1.7 fusion.19
  411.8 3.7 fusion
  415.5 20.9 %all_to_all.15 = bf16[8,32,2048]{2,1,0:T(8,128)(2,1)S(1)} all-to-all(bf16[8,32,2048]{2,1,0:T(8,128)(2,1)} %bitcast.118), channel_id=1, replica_groups=mesh['sp'=16,'fs'=4,'tp'=8] {'tp'}, dimensions={0} | all-to-all | bytes 2097152 | tf_op jit(solution)/shard_map/all_to_all | solution.py:70
  (82 shorter events, 13.9 us)
Async XLA Ops:
  8.5 20.2 %all-to-all-start.1 = ((bf16[8,32,2048]{2,1,0:T(8,128)(2,1)}), bf16[8,32,2048]{2,1,0:T(8,128)(2,1)S(1)}, u32[]{:S(2)}, u32[]{:S(2)}) async-start(bf16[8,32,2048]{2,1,0:T(8,128)(2,1)} %broadcast_in_dim.41), calls=%async_computation.1 | async-start | bytes 2097152 | tf_op jit(solution)/shard_map/all_to_all | solution.py:30
  32.2 12.7 %copy-start.2 = (f32[1,2,256]{2,1,0:T(2,128)S(1)}, f32[1,2,256]{2,1,0:T(2,128)}, u32[]{:S(2)}) copy-start(f32[1,2,256]{2,1,0:T(2,128)} %param.27) | copy-start | bytes 6148
  32.2 286.5 %copy-start.5 = (f32[256]{0:T(256)S(1)}, f32[256]{0:T(256)}, u32[]{:S(2)}) copy-start(f32[256]{0:T(256)} %param.26) | copy-start | bytes 3076
  32.2 284.8 %all-to-all-start = ((bf16[64,32,1536]{2,1,0:T(8,128)(2,1)}), bf16[64,32,1536]{2,1,0:T(8,128)(2,1)}, u32[]{:S(2)}, u32[]{:S(2)}) async-start(bf16[64,32,1536]{2,1,0:T(8,128)(2,1)} %stack.2), calls=%async_computation | async-start | bytes 12582912 | tf_op jit(solution)/shard_map/all_to_all | solution.py:17
  44.8 347.8 %all-gather.5.cloned.1.call-start = ((), (), s32[]{:S(2)}) async-start(), calls=%async_computation.3 | async-start | bytes 2228224 | tf_op jit(solution)/shard_map/all_gather | solution.py:46
  318.7 4.5 %copy-start.3 = (f32[3,128]{1,0:T(4,128)S(1)}, f32[3,128]{1,0:T(4,128)}, u32[]{:S(2)}) copy-start(f32[3,128]{1,0:T(4,128)} %param.30) | copy-start | bytes 4612
  322.5 0.7 copy-start
  322.5 86.3 %copy-start.1 = (f32[1,2,128,128]{3,2,1,0:T(8,128)S(1)}, f32[1,2,128,128]{3,2,1,0:T(8,128)}, u32[]{:S(2)}) copy-start(f32[1,2,128,128]{3,2,1,0:T(8,128)} %param.28) | copy-start | bytes 393220
  325.0 85.1 %copy-start.4 = (f32[256]{0:T(256)S(1)}, f32[256]{0:T(256)}, u32[]{:S(2)}) copy-start(f32[256]{0:T(256)} %param.29) | copy-start | bytes 3076
  329.2 82.6 %collective-permute-start = (f32[2,128]{0,1:T(8,128)}, f32[2,128]{0,1:T(8,128)}, u32[]{:S(2)}, u32[]{:S(2)}) collective-permute-start(f32[2,128]{0,1:T(8,128)} %slice.29), channel_id=1, source_target_pairs={{0,32},{32,64},{64,96},{96,128},{128,160},{160,192},{192,224},{224... | collective-permute-start | bytes 3080 | tf_op jit(solution)/shard_map/ppermute | solution.py:60
Sparse Core Ops, SparseCore 0:
  323.3 69.2 all-gather.4
